TPU v7x, 256 devices: a whole 4x4x8 slice. The times are simulated.
256 devices in a mesh: sp: 32 (over z, x), tp: 8 (over y, core).
Axes of the slice: x: 4, y: 4, z: 8, core: 2. Of those that a mesh axis runs over, the one named last changes fastest.
Arguments:
- tokens: bfloat16 [12288, 2048], P('sp', 'tp'), may hold values from -6 to 6
- pre_gain: float32 [2048], replicated, may hold values from 0.1 to 1.9
- outer_gate_weight: bfloat16 [2048, 1024], P(None, 'tp'), may hold values from -0.125 to 0.125
- inner_gate_weight: bfloat16 [2048, 1024], P(None, 'tp'), may hold values from -0.125 to 0.125
- source_weight: bfloat16 [2048, 1024], P(None, 'tp'), may hold values from -0.125 to 0.125
- conv_taps: bfloat16 [3, 1024], P(None, 'tp'), may hold values from -3.5 to 3.5
- q_down_weight: bfloat16 [2048, 768], replicated, may hold values from -0.125 to 0.125
- q_norm_gain: float32 [768], replicated, may hold values from 0.5 to 16
- q_up_weight: bfloat16 [768, 3072], P(None, 'tp'), may hold values from -0.21875 to 0.21875
- kv_down_weight: bfloat16 [2048, 512], replicated, may hold values from -0.125 to 0.125
- rope_key_weight: bfloat16 [2048, 32], replicated, may hold values from -0.125 to 0.125
- kv_norm_gain: float32 [512], replicated, may hold values from 0.5 to 16
- kv_up_weight: bfloat16 [512, 4096], P(None, 'tp'), may hold values from -0.25 to 0.25
- attn_out_weight: bfloat16 [2048, 2048], P('tp'), may hold values from -4 to 4
- conv_out_weight: bfloat16 [1024, 2048], P('tp'), may hold values from -0.1875 to 0.1875
- post_gain: float32 [2048], P('tp'), may hold values from 0.1 to 1.9
Outputs:
- mixed: bfloat16 [12288, 2048], P('sp', 'tp')
- log_total: float32 [32, 12288], P('tp', 'sp')
All inputs are finite; a program needn't handle non-finite values.
Results may differ from a plain program's by a relative error of at most 0.017.
The roundings to bfloat16 on the way count: a program that leaves them out, or rounds other values in their place, can miss the bound.
Values may be sent and summed in bfloat16 or wider, within the bound.
A program may use at most 128 MiB of HBM per device.

v0:
```python
import jax
import jax.numpy as jnp
from jax import lax
from jax.sharding import PartitionSpec as P

D = 2048
NOPE = 64
ROPE = 32
VDIM = 64
TAPS = 3


EPSILON = 1e-06
THETA = 500000.0
NEGATIVE = -1e30


def in_order(pieces, dim):
    lengths = list(pieces.shape[1:])
    lengths[dim] *= pieces.shape[0]
    return jnp.moveaxis(pieces, 0, dim).reshape(lengths)


def copy_for_each(shard, axis):
    peers = lax.axis_size(axis)
    return lax.all_to_all(
        jnp.broadcast_to(shard[None], (peers, *shard.shape)), axis, 0, 0, tiled=True
    )


def gathered_copies(shard, axis, dim):
    return in_order(copy_for_each(shard, axis), dim)


def from_behind(value, axis, steps):
    count = lax.axis_size(axis)
    leading, last = (max(0, -steps), min(count, count - steps))
    return lax.ppermute(value, axis, [(source, source + steps) for source in range(leading, last)])


def cut_along(shard, dim, peers):
    lengths = shard.shape
    pieces = shard.reshape(*lengths[:dim], peers, lengths[dim] // peers, *lengths[dim + 1 :])
    return jnp.moveaxis(pieces, dim, 0)


def summed_on_arrival(shard, axis, dim):
    peers = lax.axis_size(axis)
    pieces = lax.all_to_all(cut_along(shard, dim, peers), axis, 0, 0, tiled=True)
    return jnp.sum(pieces.astype(jnp.float32), axis=0)


def over_copies(shard, axis):
    return copy_for_each(shard, axis).sum(axis=0)


def rms_factor(values):
    return lax.rsqrt(jnp.mean(values * values, axis=-1, keepdims=True) + EPSILON)


def rotation(positions, width):
    freqs = THETA ** (-jnp.arange(0, width, 2, dtype=jnp.float32) / width)
    angles = positions.astype(jnp.float32)[:, None] * freqs[None, :]
    return (jnp.cos(angles), jnp.sin(angles))


def rotate(values, cosine, sine):
    half = values.shape[-1] // 2
    first = values[..., :half]
    second = values[..., half:]
    return jnp.concatenate(
        [first * cosine - second * sine, second * cosine + first * sine], axis=-1
    )


def block_count(rows):
    count = 1
    while rows // count > 1024 or rows % count != 0:
        count += 1
    return count


def attend(
    state, query_plain, query_turned, key_plain, values, key_turned, key_start, query_pos, scale
):
    maxima, totals, weighted = state
    rows = key_plain.shape[0]
    scores = jnp.einsum("thd,nhd->htn", query_plain, key_plain, preferred_element_type=jnp.float32)
    scores = scores + jnp.einsum(
        "thr,nr->htn", query_turned, key_turned, preferred_element_type=jnp.float32
    )
    key_pos = key_start + jnp.arange(rows, dtype=jnp.int32)
    allowed = key_pos[None, :] <= query_pos[:, None]
    scores = jnp.where(allowed[None], scores * scale, NEGATIVE)
    fresh = jnp.maximum(maxima, jnp.max(scores, axis=-1))
    shrink = jnp.exp(maxima - fresh)
    weights = jnp.exp(scores - fresh[..., None])
    totals = totals * shrink + jnp.sum(weights, axis=-1)
    weighted = weighted * shrink[..., None] + jnp.einsum(
        "htn,nhd->htd", weights.astype(jnp.bfloat16), values, preferred_element_type=jnp.float32
    )
    return (fresh, totals, weighted)


def body(
    tokens,
    pre_gain,
    outer_gate_weight,
    inner_gate_weight,
    source_weight,
    conv_taps,
    q_down_weight,
    q_norm_gain,
    q_up_weight,
    kv_down_weight,
    rope_key_weight,
    kv_norm_gain,
    kv_up_weight,
    attn_out_weight,
    conv_out_weight,
    post_gain,
):
    token_rows = tokens.shape[0]
    weights_in = (
        outer_gate_weight,
        inner_gate_weight,
        source_weight,
        q_down_weight,
        kv_down_weight,
        rope_key_weight,
    )
    wide = gathered_copies(tokens, "tp", 1).astype(jnp.float32)
    scaled = (wide * pre_gain).astype(jnp.bfloat16)
    squares = jnp.sum(wide * wide, axis=1)
    sums = tuple(
        (jnp.dot(scaled, weight, preferred_element_type=jnp.float32) for weight in weights_in)
    )
    squares, sums = (squares, sums)
    factor = lax.rsqrt(squares / D + EPSILON)[:, None]
    outer_sum, inner_sum, source_sum, q_sum, kv_sum, rope_sum = sums
    outer = (outer_sum * factor).astype(jnp.bfloat16)
    inner = (inner_sum * factor).astype(jnp.bfloat16)
    source = (source_sum * factor).astype(jnp.bfloat16)
    driven = (inner.astype(jnp.float32) * source.astype(jnp.float32)).astype(jnp.bfloat16)
    prior = from_behind(driven[token_rows - (TAPS - 1) :], "sp", 1)
    extended = jnp.concatenate([prior, driven], axis=0)
    convolved = jnp.zeros(driven.shape, jnp.float32)
    for index in range(TAPS):
        convolved = convolved + conv_taps[index].astype(jnp.float32) * extended[
            index : index + token_rows
        ].astype(jnp.float32)
    conv_branch = (outer.astype(jnp.float32) * convolved).astype(jnp.bfloat16)
    local_heads = q_up_weight.shape[1] // (NOPE + ROPE)
    query_pos = lax.axis_index("sp") * token_rows + jnp.arange(token_rows, dtype=jnp.int32)
    last_pos = lax.axis_index("sp") * token_rows + token_rows - 1
    cosine, sine = rotation(query_pos, ROPE)
    q_latent = q_sum * factor
    q_normed = (q_latent * rms_factor(q_latent) * q_norm_gain).astype(jnp.bfloat16)
    query = jnp.dot(q_normed, q_up_weight, preferred_element_type=jnp.float32)
    query = query.reshape(token_rows, local_heads, NOPE + ROPE)
    q_plain = query[..., :NOPE].astype(jnp.bfloat16)
    q_turned = rotate(query[..., NOPE:], cosine[:, None], sine[:, None]).astype(jnp.bfloat16)
    kv_latent = kv_sum * factor
    latent = (kv_latent * rms_factor(kv_latent) * kv_norm_gain).astype(jnp.bfloat16)
    rope_key = rotate(rope_sum * factor, cosine, sine).astype(jnp.bfloat16)
    scale = (NOPE + ROPE) ** (-0.5)

    def split_keys(flat):
        shaped = flat.reshape(flat.shape[0], local_heads, NOPE + VDIM)
        return (shaped[..., :NOPE], shaped[..., NOPE:])

    start_state = (
        jnp.full((local_heads, token_rows), NEGATIVE, jnp.float32),
        jnp.zeros((local_heads, token_rows), jnp.float32),
        jnp.zeros((local_heads, token_rows, VDIM), jnp.float32),
    )
    keyvals = jnp.dot(latent, kv_up_weight, preferred_element_type=jnp.float32).astype(jnp.bfloat16)
    pieces = (
        lax.all_gather(keyvals, "sp", axis=0, tiled=True),
        lax.all_gather(rope_key, "sp", axis=0, tiled=True),
    )
    rows = pieces[0].shape[0]
    count = block_count(rows)
    size = rows // count

    def advance(index, current_state):
        offset = index * size

        def compute(current):
            block = tuple((lax.dynamic_slice_in_dim(member, offset, size, 0) for member in pieces))
            key_plain, values = split_keys(block[0])
            return attend(
                current, q_plain, q_turned, key_plain, values, block[1], offset, query_pos, scale
            )

        return lax.cond(offset <= last_pos, compute, lambda current: current, current_state)

    final = lax.fori_loop(0, count, advance, start_state)
    maxima, totals, weighted = final
    log_total = maxima + jnp.log(totals)
    attended = (weighted / totals[..., None]).astype(jnp.bfloat16)
    out_rows = attn_out_weight.reshape(local_heads, VDIM, attn_out_weight.shape[1])
    partial_value = jnp.einsum(
        "htd,hdk->tk", attended, out_rows, preferred_element_type=jnp.float32
    )
    partial_value = partial_value + jnp.dot(
        conv_branch, conv_out_weight, preferred_element_type=jnp.float32
    )
    summed = summed_on_arrival(partial_value.astype(jnp.bfloat16), "tp", 1)
    row_squares = over_copies(jnp.sum(summed * summed, axis=1), "tp")
    mixed = summed * lax.rsqrt(row_squares / D + EPSILON)[:, None] * post_gain
    return (mixed.astype(jnp.bfloat16), log_total)


def solution(mesh):
    placed = (
        P("sp", "tp"),
        P(),
        P(None, "tp"),
        P(None, "tp"),
        P(None, "tp"),
        P(None, "tp"),
        P(),
        P(),
        P(None, "tp"),
        P(),
        P(),
        P(),
        P(None, "tp"),
        P("tp", None),
        P("tp", None),
        P("tp"),
    )
    return jax.shard_map(
        body, mesh=mesh, in_specs=placed, out_specs=(P("sp", "tp"), P("tp", "sp")), check_vma=False
    )
```

profile of v0, /device:TPU:226, one launch (start us, length us, event | category | flops | bytes accessed | tf_op | source)
XLA Modules:
  0.0 309.3 jit_solution(4278169343933248280)
XLA Ops:
  8.6 25.9 %all_to_all.16 = bf16[8,384,256]{1,2,0:T(8,128)(2,1)S(1)} all-to-all(bf16[8,384,256]{1,2,0:T(8,128)(2,1)S(1)} %broadcast_in_dim.21), channel_id=1, replica_groups=mesh['sp'=32,'tp'=8] {'tp'}, dimensions={0} | all-to-all | bytes 3145728 | tf_op jit(solution)/shard_map/all_to_all | solution.py:26
  39.5 3.0 multiply_reduce_fusion.1
  45.2 3.4 %collective-permute-start = (bf16[2,128]{1,0:T(2,128)(2,1)S(1)}, bf16[2,128]{1,0:T(2,128)(2,1)S(1)}, u32[]{:S(2)}, u32[]{:S(2)}) collective-permute-start(bf16[2,128]{1,0:T(2,128)(2,1)S(1)} %slice.61), channel_id=1, source_target_pairs={{0,8},{8,16},{16,24},{24,32},{32,40},{40,48},{48,56},{56,64},{64,7... | collective-permute-start | bytes 1544 | tf_op jit(solution)/shard_map/ppermute | solution.py:38
  49.2 52.3 %all_gather.7 = bf16[12288,32]{0,1:T(8,128)(2,1)} all-gather(bf16[384,32]{0,1:T(8,128)(2,1)S(1)} %pad_maximum_fusion.3), channel_id=1, replica_groups=mesh['sp'=32,'tp'=8] {'sp'}, dimensions={0}, use_global_device_ids=true | all-gather | bytes 811008 | tf_op jit(solution)/shard_map/all_gather | solution.py:180
  101.5 52.2 %all-gather.2.cloned.1.call-done = bf16[12288,512]{1,0:T(8,128)(2,1)} async-done(((bf16[384,512]{1,0:T(8,128)(2,1)}), bf16[12288,512]{1,0:T(8,128)(2,1)}) %all-gather.2.cloned.1.call-update) | async-done | bytes 12582928 | tf_op jit(solution)/shard_map/all_gather | solution.py:179
  153.7 16.7 %copy.33 = bf16[12288,512]{0,1:T(8,128)(2,1)} copy(bf16[12288,512]{1,0:T(8,128)(2,1)} %all-gather.2.cloned.1.call-done) | data formatting | bytes 25165824
  170.4 86.0 %while.18 = (s32[]{:T(128)}, f32[4,384]{1,0:T(4,128)S(1)}, f32[4,384]{1,0:T(4,128)S(1)}, f32[4,384,64]{1,2,0:T(8,128)S(1)}, s32[]{:T(128)}, /*index=5*/bf16[1228...) while((s32[]{:T(128)}, f32[4,384]{1,0:T(4,128)S(1)}, ...), condition=%wide.region_8.9_spmd.clone, body=%wide.region_3.8_spmd.clone.sunk | while | flops 516493696 | bytes 36649296 | solution.py:198
  170.4 7.1 %conditional.3 = ((f32[4,384]{1,0:T(4,128)S(1)}, f32[4,384]{1,0:T(4,128)S(1)}, f32[4,384,64]{1,2,0:T(8,128)S(1)})) conditional(s32[]{:T(128)} %convert_element_type.190, (f32[4,384]{1,0:T(4,128)S(1)}, f32[4,384]{1,0:T(4,128)S(1)}, f32[4,384,64]{1,2,0:T(8,128)S(1)}) %tuple.62, (s32[]{:T(128)}, s32[]{:T(128)}, bf16[12288,512]{0,1:T(8,128)(2,1)}, ...), branch_computations={%region_4.0_spmd, %region_5.7_spmd} | conditional | flops 516493696 | bytes 36647504 | solution.py:196
  177.6 7.1 %conditional.3 = ((f32[4,384]{1,0:T(4,128)S(1)}, f32[4,384]{1,0:T(4,128)S(1)}, f32[4,384,64]{1,2,0:T(8,128)S(1)})) conditional(s32[]{:T(128)} %convert_element_type.190, (f32[4,384]{1,0:T(4,128)S(1)}, f32[4,384]{1,0:T(4,128)S(1)}, f32[4,384,64]{1,2,0:T(8,128)S(1)}) %tuple.62, (s32[]{:T(128)}, s32[]{:T(128)}, bf16[12288,512]{0,1:T(8,128)(2,1)}, ...), branch_computations={%region_4.0_spmd, %region_5.7_spmd} | conditional | flops 516493696 | bytes 36647504 | solution.py:196
  184.8 7.1 %conditional.3 = ((f32[4,384]{1,0:T(4,128)S(1)}, f32[4,384]{1,0:T(4,128)S(1)}, f32[4,384,64]{1,2,0:T(8,128)S(1)})) conditional(s32[]{:T(128)} %convert_element_type.190, (f32[4,384]{1,0:T(4,128)S(1)}, f32[4,384]{1,0:T(4,128)S(1)}, f32[4,384,64]{1,2,0:T(8,128)S(1)}) %tuple.62, (s32[]{:T(128)}, s32[]{:T(128)}, bf16[12288,512]{0,1:T(8,128)(2,1)}, ...), branch_computations={%region_4.0_spmd, %region_5.7_spmd} | conditional | flops 516493696 | bytes 36647504 | solution.py:196
  191.9 7.1 %conditional.3 = ((f32[4,384]{1,0:T(4,128)S(1)}, f32[4,384]{1,0:T(4,128)S(1)}, f32[4,384,64]{1,2,0:T(8,128)S(1)})) conditional(s32[]{:T(128)} %convert_element_type.190, (f32[4,384]{1,0:T(4,128)S(1)}, f32[4,384]{1,0:T(4,128)S(1)}, f32[4,384,64]{1,2,0:T(8,128)S(1)}) %tuple.62, (s32[]{:T(128)}, s32[]{:T(128)}, bf16[12288,512]{0,1:T(8,128)(2,1)}, ...), branch_computations={%region_4.0_spmd, %region_5.7_spmd} | conditional | flops 516493696 | bytes 36647504 | solution.py:196
  199.1 7.1 %conditional.3 = ((f32[4,384]{1,0:T(4,128)S(1)}, f32[4,384]{1,0:T(4,128)S(1)}, f32[4,384,64]{1,2,0:T(8,128)S(1)})) conditional(s32[]{:T(128)} %convert_element_type.190, (f32[4,384]{1,0:T(4,128)S(1)}, f32[4,384]{1,0:T(4,128)S(1)}, f32[4,384,64]{1,2,0:T(8,128)S(1)}) %tuple.62, (s32[]{:T(128)}, s32[]{:T(128)}, bf16[12288,512]{0,1:T(8,128)(2,1)}, ...), branch_computations={%region_4.0_spmd, %region_5.7_spmd} | conditional | flops 516493696 | bytes 36647504 | solution.py:196
  206.3 7.1 %conditional.3 = ((f32[4,384]{1,0:T(4,128)S(1)}, f32[4,384]{1,0:T(4,128)S(1)}, f32[4,384,64]{1,2,0:T(8,128)S(1)})) conditional(s32[]{:T(128)} %convert_element_type.190, (f32[4,384]{1,0:T(4,128)S(1)}, f32[4,384]{1,0:T(4,128)S(1)}, f32[4,384,64]{1,2,0:T(8,128)S(1)}) %tuple.62, (s32[]{:T(128)}, s32[]{:T(128)}, bf16[12288,512]{0,1:T(8,128)(2,1)}, ...), branch_computations={%region_4.0_spmd, %region_5.7_spmd} | conditional | flops 516493696 | bytes 36647504 | solution.py:196
  213.4 7.1 %conditional.3 = ((f32[4,384]{1,0:T(4,128)S(1)}, f32[4,384]{1,0:T(4,128)S(1)}, f32[4,384,64]{1,2,0:T(8,128)S(1)})) conditional(s32[]{:T(128)} %convert_element_type.190, (f32[4,384]{1,0:T(4,128)S(1)}, f32[4,384]{1,0:T(4,128)S(1)}, f32[4,384,64]{1,2,0:T(8,128)S(1)}) %tuple.62, (s32[]{:T(128)}, s32[]{:T(128)}, bf16[12288,512]{0,1:T(8,128)(2,1)}, ...), branch_computations={%region_4.0_spmd, %region_5.7_spmd} | conditional | flops 516493696 | bytes 36647504 | solution.py:196
  220.6 7.1 %conditional.3 = ((f32[4,384]{1,0:T(4,128)S(1)}, f32[4,384]{1,0:T(4,128)S(1)}, f32[4,384,64]{1,2,0:T(8,128)S(1)})) conditional(s32[]{:T(128)} %convert_element_type.190, (f32[4,384]{1,0:T(4,128)S(1)}, f32[4,384]{1,0:T(4,128)S(1)}, f32[4,384,64]{1,2,0:T(8,128)S(1)}) %tuple.62, (s32[]{:T(128)}, s32[]{:T(128)}, bf16[12288,512]{0,1:T(8,128)(2,1)}, ...), branch_computations={%region_4.0_spmd, %region_5.7_spmd} | conditional | flops 516493696 | bytes 36647504 | solution.py:196
  227.8 7.1 %conditional.3 = ((f32[4,384]{1,0:T(4,128)S(1)}, f32[4,384]{1,0:T(4,128)S(1)}, f32[4,384,64]{1,2,0:T(8,128)S(1)})) conditional(s32[]{:T(128)} %convert_element_type.190, (f32[4,384]{1,0:T(4,128)S(1)}, f32[4,384]{1,0:T(4,128)S(1)}, f32[4,384,64]{1,2,0:T(8,128)S(1)}) %tuple.62, (s32[]{:T(128)}, s32[]{:T(128)}, bf16[12288,512]{0,1:T(8,128)(2,1)}, ...), branch_computations={%region_4.0_spmd, %region_5.7_spmd} | conditional | flops 516493696 | bytes 36647504 | solution.py:196
  234.9 7.1 %conditional.3 = ((f32[4,384]{1,0:T(4,128)S(1)}, f32[4,384]{1,0:T(4,128)S(1)}, f32[4,384,64]{1,2,0:T(8,128)S(1)})) conditional(s32[]{:T(128)} %convert_element_type.190, (f32[4,384]{1,0:T(4,128)S(1)}, f32[4,384]{1,0:T(4,128)S(1)}, f32[4,384,64]{1,2,0:T(8,128)S(1)}) %tuple.62, (s32[]{:T(128)}, s32[]{:T(128)}, bf16[12288,512]{0,1:T(8,128)(2,1)}, ...), branch_computations={%region_4.0_spmd, %region_5.7_spmd} | conditional | flops 516493696 | bytes 36647504 | solution.py:196
  242.1 7.1 %conditional.3 = ((f32[4,384]{1,0:T(4,128)S(1)}, f32[4,384]{1,0:T(4,128)S(1)}, f32[4,384,64]{1,2,0:T(8,128)S(1)})) conditional(s32[]{:T(128)} %convert_element_type.190, (f32[4,384]{1,0:T(4,128)S(1)}, f32[4,384]{1,0:T(4,128)S(1)}, f32[4,384,64]{1,2,0:T(8,128)S(1)}) %tuple.62, (s32[]{:T(128)}, s32[]{:T(128)}, bf16[12288,512]{0,1:T(8,128)(2,1)}, ...), branch_computations={%region_4.0_spmd, %region_5.7_spmd} | conditional | flops 516493696 | bytes 36647504 | solution.py:196
  249.3 7.1 %conditional.3 = ((f32[4,384]{1,0:T(4,128)S(1)}, f32[4,384]{1,0:T(4,128)S(1)}, f32[4,384,64]{1,2,0:T(8,128)S(1)})) conditional(s32[]{:T(128)} %convert_element_type.190, (f32[4,384]{1,0:T(4,128)S(1)}, f32[4,384]{1,0:T(4,128)S(1)}, f32[4,384,64]{1,2,0:T(8,128)S(1)}) %tuple.62, (s32[]{:T(128)}, s32[]{:T(128)}, bf16[12288,512]{0,1:T(8,128)(2,1)}, ...), branch_computations={%region_4.0_spmd, %region_5.7_spmd} | conditional | flops 516493696 | bytes 36647504 | solution.py:196
  256.4 3.5 %fusion.35 = f32[384,2048,1]{1,0,2:T(8,128)} fusion(bf16[4,64,2048]{2,1,0:T(8,128)(2,1)} %bitcast.64, f32[4,384,64]{1,2,0:T(8,128)S(1)} %get-tuple-element.215, f32[4,384]{1,0:T(4,128)S(1)} %get-tuple-element.216), kind=kOutput, calls=%fused_computation.59 | convolution fusion | flops 402849792 | bytes 4593664 | tf_op jit(solution)/shard_map/htd,hdk->tk/dot_general | solution.py:203
  259.9 4.0 %fusion.19 = bf16[384,2048]{1,0:T(8,128)(2,1)S(1)} fusion(f32[384,2048,1]{1,0,2:T(8,128)} %fusion.35, bf16[128,2048]{1,0:T(8,128)(2,1)} %param.34, bf16[384,2048]{0,1:T(8,128)(2,1)S(1)} %copy-done.3, bf16[2048,128]{1,0:T(8,128)(2,1)} %param.22, bf16[384,128]{1,0:T(8,128)(2,1)S(1)} %fusion.25, bf16[2,128]{1,0:T(2,128)(2,1)S(1)} %collective-permute-done, ...), kind=kOutput, calls=%fused_computation.25 | convolution fusion | flops 405159936 | bytes 7441920 | tf_op jit(solution)/shard_map/dot_general | solution.py:206
  264.1 25.9 %all_to_all.17 = bf16[8,384,256]{2,1,0:T(8,128)(2,1)S(1)} all-to-all(bf16[8,384,256]{2,1,0:T(8,128)(2,1)S(1)} %bitcast.60), channel_id=1, replica_groups=mesh['sp'=32,'tp'=8] {'tp'}, dimensions={0} | all-to-all | bytes 3145728 | tf_op jit(solution)/shard_map/all_to_all | solution.py:49
  291.0 3.9 %all-to-all-start.2 = ((f32[8,1,384]{2,1,0:T(1,128)}), f32[8,1,384]{2,1,0:T(1,128)}, u32[]{:S(2)}, u32[]{:S(2)}) async-start(f32[8,1,384]{2,1,0:T(1,128)} %broadcast_in_dim.22), calls=%async_computation.2 | async-start | bytes 24576 | tf_op jit(solution)/shard_map/all_to_all | solution.py:26
  295.5 4.7 %all-to-all-done.2 = f32[8,1,384]{2,1,0:T(1,128)} async-done(((f32[8,1,384]{2,1,0:T(1,128)}), f32[8,1,384]{2,1,0:T(1,128)}, u32[]{:S(2)}, u32[]{:S(2)}) %all-to-all-start.2) | async-done | bytes 12320 | tf_op jit(solution)/shard_map/all_to_all | solution.py:26
  (208 shorter events, 98.1 us)
Async XLA Ops:
  7.2 32.3 %copy-start = (bf16[2048,768]{1,0:T(8,128)(2,1)S(1)}, bf16[2048,768]{1,0:T(8,128)(2,1)}, u32[]{:S(2)}) copy-start(bf16[2048,768]{1,0:T(8,128)(2,1)} %param.26) | copy-start | bytes 9437188
  7.2 146.5 %all-gather.2.cloned.1.call-start = ((), (), s32[]{:S(2)}) async-start(), calls=%async_computation.3 | async-start | bytes 12976128 | tf_op jit(solution)/shard_map/all_gather | solution.py:179
  34.5 0.7 copy-start.9
  35.2 1.6 copy-start.13
  36.8 1.1 copy-start.2
  36.8 1.4 copy-start.5
  36.8 1.4 copy-start.12
  37.9 1.5 copy-start.11
  39.4 3.0 copy-start.4
  39.5 3.0 copy-start.10
  42.4 1.4 copy-start.3
  42.5 1.5 copy-start.6
  43.1 1.5 copy-start.7
  44.6 4.1 %copy-start.8 = (bf16[2048,32]{0,1:T(8,128)(2,1)S(1)}, bf16[2048,32]{0,1:T(8,128)(2,1)}, u32[]{:S(2)}) copy-start(bf16[2048,32]{0,1:T(8,128)(2,1)} %param.30) | copy-start | bytes 393220
  45.2 214.7 %collective-permute-start = (bf16[2,128]{1,0:T(2,128)(2,1)S(1)}, bf16[2,128]{1,0:T(2,128)(2,1)S(1)}, u32[]{:S(2)}, u32[]{:S(2)}) collective-permute-start(bf16[2,128]{1,0:T(2,128)(2,1)S(1)} %slice.61), channel_id=1, source_target_pairs={{0,8},{8,16},{16,24},{24,32},{32,40},{40,48},{48,56},{56,64},{64,7... | collective-permute-start | bytes 1544 | tf_op jit(solution)/shard_map/ppermute | solution.py:38
  264.0 38.5 %copy-start.1 = (bf16[2048,768]{1,0:T(8,128)(2,1)S(1)}, bf16[2048,768]{1,0:T(8,128)(2,1)}, u32[]{:S(2)}) copy-start(bf16[2048,768]{1,0:T(8,128)(2,1)} %param.26) | copy-start | bytes 9437188
  291.0 9.3 %all-to-all-start.2 = ((f32[8,1,384]{2,1,0:T(1,128)}), f32[8,1,384]{2,1,0:T(1,128)}, u32[]{:S(2)}, u32[]{:S(2)}) async-start(f32[8,1,384]{2,1,0:T(1,128)} %broadcast_in_dim.22), calls=%async_computation.2 | async-start | bytes 24576 | tf_op jit(solution)/shard_map/all_to_all | solution.py:26
Sparse Core Ops, SparseCore 0:
  39.5 114.1 all-gather.1
where the time goes:
time: 311 us; the launch traced here: 309 us
  blocking collectives  104 us (33%)
  matrix products  70.1 us (23%)
  waiting for transfers between devices  56.9 us (18%)
  local copies, waits for them, and re-layouts  37.2 us (12%)
  other arithmetic  17.9 us (6%)
  between operations  14.3 us (5%)
  starting transfers between devices  7.38 us (2%)
    all_gather x1, blocking collectives, body(): lax.all_gather(rope_key, 'sp', axis=0, tiled=True)  52.3 us
    all_gather x1, waiting for transfers between devices, body(): lax.all_gather(keyvals, 'sp', axis=0, tiled=True)  52.2 us
    all_to_all x1, blocking collectives, summed_on_arrival(): lax.all_to_all(cut_along(shard, dim, peers), axis, 0, 0, tiled=True)  25.9 us
    all_to_all x1, blocking collectives, copy_for_each(): lax.all_to_all(jnp.broadcast_to(shard[None], (peers, *shard.shape)), axis...  25.9 us
    dot_general x12, matrix products, attend(): jnp.einsum('thr,nr->htn', query_turned, key_turned, preferred_element_typ...  22.1 us
    unnamed x30, local copies, waits for them, and re-layouts  20.6 us
    dot_general x12, matrix products, attend(): jnp.einsum('thd,nhd->htn', query_plain, key_plain, preferred_element_type...  18.7 us
    dynamic_slice x12, local copies, waits for them, and re-layouts, compute(): lax.dynamic_slice_in_dim(member, offset, size, 0)  15.6 us
  transfers between devices with their start and end apart: 3, of which 2 were waited for; matrix products, arithmetic and copies ran while one was open for 36% of the time, Pallas kernels for 0%

commit v1 on v0

v1 whole, which is shorter than its diff:
```python
import functools
import math

import jax
import jax.numpy as jnp
from jax import lax
from jax.experimental import pallas as pl
from jax.experimental.pallas import tpu as pltpu
from jax.sharding import PartitionSpec as P

D = 2048
NOPE = 64
ROPE = 32
VDIM = 64
TAPS = 3
NZ, NX, NY = 8, 4, 4
ROWS = 384
KVR = NOPE + ROPE + VDIM
QK = NOPE + ROPE
LOCAL = 4
BLOCKS = NZ * NX

EPSILON = 1e-06
THETA = 500000.0
NEGATIVE = -1e30
LOG2E = math.log2(math.e)
MESH = pl.DeviceIdType.MESH
VMEM = pltpu.MemorySpace.VMEM


def side(z):
    return lax.rem(lax.div(z + 1, 2), 2)


def plane(j, core):
    return 2 * j + lax.rem(j + core, 2)


def remote(src, dst, send, recv, sp, tp):
    return pltpu.make_async_remote_copy(
        src_ref=src, dst_ref=dst, send_sem=send, recv_sem=recv,
        device_id=(sp, tp), device_id_type=MESH,
    )


def greet(peers):
    barrier = pltpu.get_barrier_semaphore()
    for sp, tp in peers:
        pl.semaphore_signal(barrier, inc=1, device_id=(sp, tp), device_id_type=MESH)
    pl.semaphore_wait(barrier, len(peers))


def gather_kernel(part_ref, out_ref, y_send, y_recv, d_send, d_recv):
    sp = lax.axis_index("sp")
    tp = lax.axis_index("tp")
    core = lax.rem(tp, 2)
    y = lax.div(tp, 2)
    mate = tp + 1 - 2 * core
    up = lax.rem(y + 1, NY) * 2 + core
    down = lax.rem(y + NY - 1, NY) * 2 + core
    far = lax.rem(y + 2, NY) * 2 + core
    rows, width = part_ref.shape
    half = rows // 2

    def slot(owner, first=0, count=rows):
        return out_ref.at[pl.ds(first, count), pl.ds(pl.multiple_of(owner * width, width), width)]

    greet([(sp, mate), (sp, up), (sp, down)])
    copies = []

    def send(src, dst, s, r, to):
        c = remote(src, dst, s, r, sp, to)
        c.start()
        copies.append(c)

    send(part_ref, slot(tp), y_send.at[0], y_recv.at[0], up)
    send(part_ref, slot(tp), y_send.at[1], y_recv.at[1], down)
    send(part_ref, slot(tp), d_send.at[0], d_recv.at[0], mate)
    out_ref[:, pl.ds(pl.multiple_of(tp * width, width), width)] = part_ref[...]

    def arrived(index, owner, first=0, count=rows):
        remote(slot(owner, first, count), slot(owner, first, count),
               y_send.at[index], y_recv.at[index], sp, up).wait_recv()

    arrived(0, down)
    send(slot(down, 0, half), slot(down, 0, half), y_send.at[2], y_recv.at[2], up)
    send(slot(down), slot(down), d_send.at[1], d_recv.at[1], mate)
    arrived(1, up)
    send(slot(up, half, half), slot(up, half, half), y_send.at[3], y_recv.at[3], down)
    send(slot(up), slot(up), d_send.at[2], d_recv.at[2], mate)
    arrived(2, far, 0, half)
    send(slot(far, 0, half), slot(far, 0, half), d_send.at[3], d_recv.at[3], mate)
    arrived(3, far, half, half)
    send(slot(far, half, half), slot(far, half, half), d_send.at[4], d_recv.at[4], mate)

    other = 1 - 2 * core
    for index, (owner, first, count) in enumerate(
        [(mate, 0, rows), (down + other, 0, rows), (up + other, 0, rows),
         (far + other, 0, half), (far + other, half, half)]
    ):
        remote(slot(owner, first, count), slot(owner, first, count),
               d_send.at[index], d_recv.at[index], sp, mate).wait_recv()
    for c in copies:
        c.wait_send()


def gathered(part, collective_id):
    rows, width = part.shape
    return pl.pallas_call(
        gather_kernel,
        out_shape=jax.ShapeDtypeStruct((rows, width * 2 * NY), part.dtype),
        in_specs=[pl.BlockSpec(memory_space=VMEM)],
        out_specs=pl.BlockSpec(memory_space=VMEM),
        scratch_shapes=[
            pltpu.SemaphoreType.DMA((4,)),
            pltpu.SemaphoreType.DMA((4,)),
            pltpu.SemaphoreType.DMA((5,)),
            pltpu.SemaphoreType.DMA((5,)),
        ],
        compiler_params=pltpu.CompilerParams(collective_id=collective_id, has_side_effects=True),
        name="gather_tp",
    )(part)


def exchange_kernel(kv_ref, q_ref, all_ref, mine_ref,
                    kz_send, kz_recv, qz_send, qz_recv, x_send, x_recv, d_send, d_recv):
    sp = lax.axis_index("sp")
    tp = lax.axis_index("tp")
    z, x = lax.div(sp, NX), lax.rem(sp, NX)
    core, y = lax.rem(tp, 2), lax.div(tp, 2)
    mate = tp + 1 - 2 * core
    xp, xm, xf = (lax.rem(x + k, NX) for k in (1, NX - 1, 2))
    to_core = side(z)
    owner = lax.div(z, LOCAL)
    half = KVR // 2

    peers = [(lax.rem(z + k, NZ) * NX + x, 2 * y + c) for k in range(1, NZ) for c in (0, 1)]
    peers += [(sp, mate), (z * NX + xp, tp), (z * NX + xm, tp)]
    greet(peers)

    keep = jnp.logical_and(owner == core, to_core == core)
    own_head = z - LOCAL * core

    def z_copies(h):
        target = LOCAL * core + h
        return (
            remote(kv_ref.at[h], all_ref.at[sp], kz_send.at[h], kz_recv.at[lax.div(z, 2)],
                   target * NX + x, 2 * y + to_core),
            remote(q_ref.at[h], mine_ref.at[lax.div(z, 2)], qz_send.at[h],
                   qz_recv.at[lax.div(z, 2)], target * NX + x, 2 * y + to_core),
        )

    def leaves(h):
        return jnp.logical_not(jnp.logical_and(keep, own_head == h))

    for which in (0, 1):
        for h in range(LOCAL):
            @pl.when(leaves(h))
            def _(h=h):
                z_copies(h)[which].start()

    for h in range(LOCAL):
        @pl.when(jnp.logical_not(leaves(h)))
        def _(h=h):
            all_ref[sp] = kv_ref[h]
            mine_ref[lax.div(z, 2)] = q_ref[h]

    first = lax.div(z, 2)
    order = [lax.rem(first + k, 4) for k in (0, 1, 3, 2)]
    sends = []

    def send(src, s, r, to_sp, to_tp):
        c = remote(src, src, s, r, to_sp, to_tp)
        c.start()
        sends.append(c)

    def z_wait(j, dst, send_sem, recv_sem):
        from_plane = plane(j, core)

        @pl.when(jnp.logical_not(jnp.logical_and(keep, from_plane == z)))
        def _():
            remote(dst, dst, send_sem, recv_sem, sp, mate).wait_recv()

    def z_stage(j):
        block = all_ref.at[plane(j, core) * NX + x]
        z_wait(j, block, kz_send.at[0], kz_recv.at[j])
        send(block, x_send.at[j, 0], x_recv.at[j, 0], z * NX + xp, tp)
        send(block, x_send.at[j, 1], x_recv.at[j, 1], z * NX + xm, tp)
        send(block, d_send.at[j, 0], d_recv.at[j, 0], sp, mate)

    def wait(dst, sems, index):
        remote(dst, dst, sems[0].at[index], sems[1].at[index], sp, mate).wait_recv()

    def x_stage(j):
        base = plane(j, core) * NX
        wait(all_ref.at[base + xm], (x_send, x_recv), (j, 0))
        send(all_ref.at[base + xm, pl.ds(0, half)], x_send.at[j, 2], x_recv.at[j, 2], z * NX + xp, tp)
        send(all_ref.at[base + xm], d_send.at[j, 1], d_recv.at[j, 1], sp, mate)
        wait(all_ref.at[base + xp], (x_send, x_recv), (j, 1))
        send(all_ref.at[base + xp, pl.ds(half, half)], x_send.at[j, 3], x_recv.at[j, 3], z * NX + xm, tp)
        send(all_ref.at[base + xp], d_send.at[j, 2], d_recv.at[j, 2], sp, mate)

    def far_stage(j):
        base = plane(j, core) * NX
        for k in (0, 1):
            part = all_ref.at[base + xf, pl.ds(k * half, half)]
            wait(part, (x_send, x_recv), (j, 2 + k))
            send(part, d_send.at[j, 3 + k], d_recv.at[j, 3 + k], sp, mate)

    for step in range(6):
        if step < 4:
            z_stage(order[step])
        if 1 <= step < 5:
            x_stage(order[step - 1])
        if step >= 2:
            far_stage(order[step - 2])

    for j in range(4):
        base = plane(j, 1 - core) * NX
        wait(all_ref.at[base + x], (d_send, d_recv), (j, 0))
        wait(all_ref.at[base + xm], (d_send, d_recv), (j, 1))
        wait(all_ref.at[base + xp], (d_send, d_recv), (j, 2))
        for k in (0, 1):
            wait(all_ref.at[base + xf, pl.ds(k * half, half)], (d_send, d_recv), (j, 3 + k))
        z_wait(j, mine_ref.at[j], qz_send.at[0], qz_recv.at[j])
    for c in sends:
        c.wait_send()
    for h in range(LOCAL):
        @pl.when(leaves(h))
        def _(h=h):
            for c in z_copies(h):
                c.wait_send()


def exchanged(kv, q):
    return pl.pallas_call(
        exchange_kernel,
        out_shape=(
            jax.ShapeDtypeStruct((BLOCKS, KVR, ROWS), kv.dtype),
            jax.ShapeDtypeStruct((LOCAL, QK, ROWS), q.dtype),
        ),
        in_specs=[pl.BlockSpec(memory_space=VMEM)] * 2,
        out_specs=(pl.BlockSpec(memory_space=VMEM),) * 2,
        scratch_shapes=[
            pltpu.SemaphoreType.DMA((4,)),
            pltpu.SemaphoreType.DMA((4,)),
            pltpu.SemaphoreType.DMA((4,)),
            pltpu.SemaphoreType.DMA((4,)),
            pltpu.SemaphoreType.DMA((4, 4)),
            pltpu.SemaphoreType.DMA((4, 4)),
            pltpu.SemaphoreType.DMA((4, 5)),
            pltpu.SemaphoreType.DMA((4, 5)),
        ],
        compiler_params=pltpu.CompilerParams(collective_id=1, has_side_effects=True),
        name="heads_to_planes",
    )(kv, q)


def attention_kernel(kv_ref, q_ref, out_ref, log_ref, keys, m_ref, l_ref, acc_ref):
    sp = lax.axis_index("sp")
    core = lax.rem(lax.axis_index("tp"), 2)
    x = lax.rem(sp, NX)
    factor = QK ** -0.5 * LOG2E

    def turn(kb, carry):
        keys[kb] = kv_ref[kb, 0:QK, :].astype(jnp.float32).T.astype(jnp.bfloat16)
        return carry

    lax.fori_loop(0, BLOCKS, turn, 0)

    for j in range(LOCAL):
        own = plane(j, core) * NX + x
        m_ref[...] = jnp.full_like(m_ref, NEGATIVE)
        l_ref[...] = jnp.zeros_like(l_ref)
        acc_ref[...] = jnp.zeros_like(acc_ref)
        query = q_ref[j]

        def step(kb, masked):
            scores = jnp.dot(keys[kb], query, preferred_element_type=jnp.float32) * factor
            if masked:
                key = lax.broadcasted_iota(jnp.int32, scores.shape, 0)
                row = lax.broadcasted_iota(jnp.int32, scores.shape, 1)
                scores = jnp.where(key <= row, scores, NEGATIVE)
            old = m_ref[...]
            fresh = jnp.maximum(old, jnp.max(scores, axis=0, keepdims=True))
            shrink = jnp.exp2(old - fresh)
            weights = jnp.exp2(scores - fresh)
            m_ref[...] = fresh
            l_ref[...] = l_ref[...] * shrink + jnp.sum(weights, axis=0, keepdims=True)
            acc_ref[...] = acc_ref[...] * shrink + jnp.dot(
                kv_ref[kb, QK:KVR, :], weights.astype(jnp.bfloat16),
                preferred_element_type=jnp.float32,
            )

        def advance(kb, carry):
            step(kb, False)
            return carry

        lax.fori_loop(0, own, advance, 0)
        step(own, True)
        out_ref[j] = (acc_ref[...] / l_ref[...]).astype(jnp.bfloat16)
        total = m_ref[...] * (1.0 / LOG2E) + jnp.log(l_ref[...])
        log_ref[j] = jnp.broadcast_to(total, (8, ROWS))


def attended_heads(kv, q):
    return pl.pallas_call(
        attention_kernel,
        out_shape=(
            jax.ShapeDtypeStruct((LOCAL, VDIM, ROWS), jnp.bfloat16),
            jax.ShapeDtypeStruct((LOCAL, 8, ROWS), jnp.float32),
        ),
        in_specs=[pl.BlockSpec(memory_space=VMEM)] * 2,
        out_specs=(pl.BlockSpec(memory_space=VMEM),) * 2,
        scratch_shapes=[
            pltpu.VMEM((BLOCKS, ROWS, QK), jnp.bfloat16),
            pltpu.VMEM((1, ROWS), jnp.float32),
            pltpu.VMEM((1, ROWS), jnp.float32),
            pltpu.VMEM((VDIM, ROWS), jnp.float32),
        ],
        cost_estimate=pl.CostEstimate(flops=6 * 10**9, bytes_accessed=10**7, transcendentals=10**7),
        name="attention",
    )(kv, q)


def return_kernel(out_ref, log_ref, all_ref, logs_ref, a_send, a_recv, b_send, b_recv):
    sp = lax.axis_index("sp")
    tp = lax.axis_index("tp")
    z, x = lax.div(sp, NX), lax.rem(sp, NX)
    core, y = lax.rem(tp, 2), lax.div(tp, 2)
    mate = tp + 1 - 2 * core
    greet([(lax.rem(z + k, NZ) * NX + x, 2 * y + c) for k in range(1, NZ) for c in (0, 1)]
          + [(sp, mate)])
    to = 2 * y + lax.div(z, LOCAL)
    head = lax.rem(z, LOCAL)

    def copies(j):
        target = plane(j, core) * NX + x
        return (
            remote(out_ref.at[j], all_ref.at[head], a_send.at[j], a_recv.at[head], target, to),
            remote(log_ref.at[j], logs_ref.at[head], b_send.at[j], b_recv.at[head], target, to),
        )

    keep = jnp.logical_and(to == tp, side(z) == core)

    def leaves(j):
        return jnp.logical_not(jnp.logical_and(keep, plane(j, core) == z))

    for which in (0, 1):
        for j in range(LOCAL):
            @pl.when(leaves(j))
            def _(j=j):
                copies(j)[which].start()
    for j in range(LOCAL):
        @pl.when(jnp.logical_not(leaves(j)))
        def _(j=j):
            all_ref[head] = out_ref[j]
            logs_ref[head] = log_ref[j]
    for h in range(LOCAL):
        @pl.when(jnp.logical_not(jnp.logical_and(keep, LOCAL * core + h == z)))
        def _(h=h):
            remote(all_ref.at[h], all_ref.at[h], a_send.at[h], a_recv.at[h], sp, mate).wait_recv()
            remote(logs_ref.at[h], logs_ref.at[h], b_send.at[h], b_recv.at[h], sp, mate).wait_recv()
    for j in range(LOCAL):
        @pl.when(leaves(j))
        def _(j=j):
            for c in copies(j):
                c.wait_send()


def returned(out, log):
    return pl.pallas_call(
        return_kernel,
        out_shape=(
            jax.ShapeDtypeStruct(out.shape, out.dtype),
            jax.ShapeDtypeStruct(log.shape, log.dtype),
        ),
        in_specs=[pl.BlockSpec(memory_space=VMEM)] * 2,
        out_specs=(pl.BlockSpec(memory_space=VMEM),) * 2,
        scratch_shapes=[pltpu.SemaphoreType.DMA((4,))] * 4,
        compiler_params=pltpu.CompilerParams(collective_id=2, has_side_effects=True),
        name="results_to_rows",
    )(out, log)


def copy_for_each(shard, axis):
    peers = lax.axis_size(axis)
    return lax.all_to_all(
        jnp.broadcast_to(shard[None], (peers, *shard.shape)), axis, 0, 0, tiled=True
    )


def from_behind(value, axis, steps):
    count = lax.axis_size(axis)
    leading, last = (max(0, -steps), min(count, count - steps))
    return lax.ppermute(value, axis, [(source, source + steps) for source in range(leading, last)])


def cut_along(shard, dim, peers):
    lengths = shard.shape
    pieces = shard.reshape(*lengths[:dim], peers, lengths[dim] // peers, *lengths[dim + 1 :])
    return jnp.moveaxis(pieces, dim, 0)


def summed_on_arrival(shard, axis, dim):
    peers = lax.axis_size(axis)
    pieces = lax.all_to_all(cut_along(shard, dim, peers), axis, 0, 0, tiled=True)
    return jnp.sum(pieces.astype(jnp.float32), axis=0)


def over_copies(shard, axis):
    return copy_for_each(shard, axis).sum(axis=0)


def rms_factor(values):
    return lax.rsqrt(jnp.mean(values * values, axis=-1, keepdims=True) + EPSILON)


def rotation(positions, width):
    freqs = THETA ** (-jnp.arange(0, width, 2, dtype=jnp.float32) / width)
    angles = freqs[:, None] * positions.astype(jnp.float32)[None, :]
    return (jnp.cos(angles), jnp.sin(angles))


def rotate(values, cosine, sine):
    half = values.shape[-2] // 2
    first = values[..., :half, :]
    second = values[..., half:, :]
    return jnp.concatenate(
        [first * cosine - second * sine, second * cosine + first * sine], axis=-2
    )


def dot_turned(weight, rows):
    return lax.dot_general(
        weight, rows, (((0,), (1,)), ((), ())), preferred_element_type=jnp.float32
    )


def body(
    tokens,
    pre_gain,
    outer_gate_weight,
    inner_gate_weight,
    source_weight,
    conv_taps,
    q_down_weight,
    q_norm_gain,
    q_up_weight,
    kv_down_weight,
    rope_key_weight,
    kv_norm_gain,
    kv_up_weight,
    attn_out_weight,
    conv_out_weight,
    post_gain,
):
    token_rows = tokens.shape[0]
    wide = gathered(tokens, 0).astype(jnp.float32)
    scaled = (wide * pre_gain).astype(jnp.bfloat16)
    squares = jnp.sum(wide * wide, axis=1)
    factor = lax.rsqrt(squares / D + EPSILON)[:, None]

    def project(weight):
        return jnp.dot(scaled, weight, preferred_element_type=jnp.float32) * factor

    query_pos = lax.axis_index("sp") * token_rows + jnp.arange(token_rows, dtype=jnp.int32)
    cosine, sine = rotation(query_pos, ROPE)
    q_latent = project(q_down_weight)
    q_normed = (q_latent * rms_factor(q_latent) * q_norm_gain).astype(jnp.bfloat16)
    query = dot_turned(q_up_weight, q_normed).reshape(LOCAL, QK, token_rows)
    q_send = jnp.concatenate(
        [query[:, :NOPE], rotate(query[:, NOPE:], cosine, sine)], axis=1
    ).astype(jnp.bfloat16)
    kv_latent = project(kv_down_weight)
    latent = (kv_latent * rms_factor(kv_latent) * kv_norm_gain).astype(jnp.bfloat16)
    rope_key = rotate(project(rope_key_weight).T, cosine, sine).astype(jnp.bfloat16)
    keyvals = dot_turned(kv_up_weight, latent).astype(jnp.bfloat16)
    keyvals = keyvals.reshape(LOCAL, NOPE + VDIM, token_rows)
    kv_send = jnp.concatenate(
        [
            keyvals[:, :NOPE],
            jnp.broadcast_to(rope_key[None], (LOCAL, ROPE, token_rows)),
            keyvals[:, NOPE:],
        ],
        axis=1,
    )

    outer = project(outer_gate_weight).astype(jnp.bfloat16)
    inner = project(inner_gate_weight).astype(jnp.bfloat16)
    source = project(source_weight).astype(jnp.bfloat16)
    driven = (inner.astype(jnp.float32) * source.astype(jnp.float32)).astype(jnp.bfloat16)
    prior = from_behind(driven[token_rows - (TAPS - 1) :], "sp", 1)
    extended = jnp.concatenate([prior, driven], axis=0)
    convolved = jnp.zeros(driven.shape, jnp.float32)
    for index in range(TAPS):
        convolved = convolved + conv_taps[index].astype(jnp.float32) * extended[
            index : index + token_rows
        ].astype(jnp.float32)
    conv_branch = (outer.astype(jnp.float32) * convolved).astype(jnp.bfloat16)

    kv_all, q_mine = exchanged(kv_send, q_send)
    out, log = attended_heads(kv_all, q_mine)
    heads, logs = returned(out, log)
    log_total = logs[:, 0, :]
    attended = heads.reshape(LOCAL * VDIM, token_rows)
    partial_value = lax.dot_general(
        attended, attn_out_weight, (((0,), (0,)), ((), ())), preferred_element_type=jnp.float32
    )
    partial_value = partial_value + jnp.dot(
        conv_branch, conv_out_weight, preferred_element_type=jnp.float32
    )
    summed = summed_on_arrival(partial_value.astype(jnp.bfloat16), "tp", 1)
    row_squares = over_copies(jnp.sum(summed * summed, axis=1), "tp")
    mixed = summed * lax.rsqrt(row_squares / D + EPSILON)[:, None] * post_gain
    return (mixed.astype(jnp.bfloat16), log_total)


def solution(mesh):
    placed = (
        P("sp", "tp"),
        P(),
        P(None, "tp"),
        P(None, "tp"),
        P(None, "tp"),
        P(None, "tp"),
        P(),
        P(),
        P(None, "tp"),
        P(),
        P(),
        P(),
        P(None, "tp"),
        P("tp", None),
        P("tp", None),
        P("tp"),
    )
    return jax.shard_map(
        body, mesh=mesh, in_specs=placed, out_specs=(P("sp", "tp"), P("tp", "sp")), check_vma=False
    )
```

time: 311 us -> 190 us (0.61)
  the two profiles are of different devices: /device:TPU:226 before, /device:TPU:6 now
where the time goes in v1:
time: 190 us; the launch traced here: 189 us
  Pallas kernels  115 us (61%)
  blocking collectives  25.2 us (13%)
  matrix products  21.2 us (11%)
  other arithmetic  8.8 us (5%)
  local copies, waits for them, and re-layouts  7.52 us (4%)
  starting transfers between devices  7.06 us (4%)
  waiting for transfers between devices  3.86 us (2%)
    pallas_call x1, Pallas kernels, attended_heads(): pl.pallas_call(attention_kernel, out_shape=(jax.ShapeDtypeStruct((LOCAL,...  42.4 us
    pallas_call x1, Pallas kernels, exchanged(): pl.pallas_call(exchange_kernel, out_shape=(jax.ShapeDtypeStruct((BLOCKS,...  39.1 us
    all_to_all x1, blocking collectives, summed_on_arrival(): lax.all_to_all(cut_along(shard, dim, peers), axis, 0, 0, tiled=True)  25.2 us
    pallas_call x1, Pallas kernels, returned(): pl.pallas_call(return_kernel, out_shape=(jax.ShapeDtypeStruct(out.shape,...  17.2 us
    pallas_call x1, Pallas kernels, gathered(): pl.pallas_call(gather_kernel, out_shape=jax.ShapeDtypeStruct((rows, width...  15.8 us
    dot_general x5, matrix products, project(): return jnp.dot(scaled, weight, preferred_element_type=jnp.float32) * factor  8.63 us
    dot_general x1, matrix products, body(): jnp.dot(conv_branch, conv_out_weight, preferred_element_type=jnp.float32)  5.72 us
    all_to_all x1, waiting for transfers between devices, copy_for_each(): lax.all_to_all(jnp.broadcast_to(shard[None], (peers, *shard.shape)), axis...  3.86 us
  transfers between devices with their start and end apart: 2, of which 1 were waited for; matrix products, arithmetic and copies ran while one was open for 11% of the time, Pallas kernels for 52%

profile of v1, /device:TPU:6, one launch (start us, length us, event | category | flops | bytes accessed | tf_op | source)
XLA Modules:
  0.0 189.1 jit_solution(2933795892496020797)
XLA Ops:
  0.7 15.8 %gather_tp.1 = bf16[384,2048]{1,0:T(8,128)(2,1)} custom-call(bf16[384,256]{1,0:T(8,128)(2,1)} %part_ref.1), custom_call_target="tpu_custom_call" | custom-call | tf_op jit(solution)/shard_map/gather_tp/pallas_call | solution.py:109
  16.5 1.9 %fusion.1 = f32[384]{0:T(512)S(1)} fusion(bf16[384,2048]{1,0:T(8,128)(2,1)} %gather_tp.1), kind=kLoop, calls=%fused_computation.3 | loop fusion | flops 2358912 | bytes 1574400 | tf_op jit(solution)/shard_map/reduce_sum | solution.py:461
  18.5 1.7 fusion.9
  21.9 3.7 %collective-permute-start = (bf16[2,128]{1,0:T(2,128)(2,1)}, bf16[2,128]{1,0:T(2,128)(2,1)}, u32[]{:S(2)}, u32[]{:S(2)}) collective-permute-start(bf16[2,128]{1,0:T(2,128)(2,1)} %slice.67), channel_id=1, source_target_pairs={{0,8},{8,16},{16,24},{24,32},{32,40},{40,48},{48,56},{56,64},{64,7... | collective-permute-start | bytes 1544 | tf_op jit(solution)/shard_map/ppermute | solution.py:396
  26.2 2.4 %multiply_reduce_fusion = (f32[384]{0:T(512)S(1)}, f32[384,768]{1,0:T(8,128)}) fusion(f32[384]{0:T(512)S(1)} %add_rsqrt_fusion.3, bf16[2048,768]{1,0:T(8,128)(2,1)S(1)} %copy-done, bf16[384,2048]{1,0:T(8,128)(2,1)S(1)} %copy-done.1, f32[2048]{0:T(1024)S(1)} %copy-done.7), kind=kOutput, calls=%fused_computation.12 | convolution fusion | flops 1211203200 | bytes 5909504 | tf_op jit(solution)/shard_map/dot_general | solution.py:465
  28.6 1.2 fusion.13
  29.8 2.1 %fusion.21 = f32[384,384]{0,1:T(8,128)S(1)} fusion(bf16[768,384]{1,0:T(8,128)(2,1)} %param.24, f32[384,768]{1,0:T(8,128)} %get-tuple-element.30, f32[768]{0:T(1024)S(1)} %copy-done.8, f32[384]{0:T(512)S(1)} %add_rsqrt_fusion.1), kind=kOutput, calls=%fused_computation.30 | convolution fusion | flops 227377152 | bytes 2363904 | tf_op jit(solution)/shard_map/dot_general | solution.py:435
  33.5 2.7 %multiply_reduce_fusion.1 = (f32[384]{0:T(512)S(1)}, f32[384,512]{1,0:T(8,128)S(1)}) fusion(f32[384]{0:T(512)S(1)} %add_rsqrt_fusion.3, bf16[2048,512]{1,0:T(8,128)(2,1)} %param.25, bf16[384,2048]{1,0:T(8,128)(2,1)S(1)} %copy-done.2, f32[2048]{0:T(1024)S(1)} %copy-done.7), kind=kOutput, calls=%fused_computation.29 | convolution fusion | flops 808255104 | bytes 4467712 | tf_op jit(solution)/shard_map/dot_general | solution.py:465
  36.3 1.2 fusion.2
  37.4 1.2 copy.23
  38.7 0.9 multiply_cosine_fusion
  39.6 1.0 subtract_convert_fusion
  40.6 1.7 pad_maximum_fusion.1.q_ref
  42.3 0.8 pad_maximum_fusion.kv_ref
  43.2 39.1 %heads_to_planes.1 = (bf16[32,160,384]{2,1,0:T(8,128)(2,1)}, bf16[4,96,384]{2,1,0:T(8,128)(2,1)}) custom-call(bf16[4,160,384]{2,1,0:T(8,128)(2,1)} %pad_maximum_fusion.kv_ref, bf16[4,96,384]{2,1,0:T(8,128)(2,1)} %pad_maximum_fusion.1.q_ref), custom_call_target="tpu_custom_call" | custom-call | tf_op jit(solution)/shard_map/heads_to_planes/pallas_call | solution.py:236
  82.3 42.4 %attention.1 = (bf16[4,64,384]{2,1,0:T(8,128)(2,1)}, f32[4,8,384]{2,1,0:T(8,128)}) custom-call(bf16[32,160,384]{2,1,0:T(8,128)(2,1)} %get-tuple-element.8.kv_ref, bf16[4,96,384]{2,1,0:T(8,128)(2,1)} %get-tuple-element.9.q_ref), custom_call_target="tpu_custom_call" | custom-call | flops 6000000000 | bytes 10000000 | tf_op jit(solution)/shard_map/attention/pallas_call | solution.py:307
  124.7 17.2 %results_to_rows.1 = (bf16[4,64,384]{2,1,0:T(8,128)(2,1)}, f32[4,8,384]{2,1,0:T(8,128)}) custom-call(bf16[4,64,384]{2,1,0:T(8,128)(2,1)} %get-tuple-element.10.out_ref, f32[4,8,384]{2,1,0:T(8,128)} %get-tuple-element.11.log_ref), custom_call_target="tpu_custom_call" | custom-call | tf_op jit(solution)/shard_map/results_to_rows/pallas_call | solution.py:372
  141.9 3.6 %fusion.43 = f32[384,2048]{1,0:T(8,128)} fusion(bf16[256,384]{1,0:T(8,128)(2,1)} %bitcast.44, bf16[256,2048]{1,0:T(8,128)(2,1)} %param.29), kind=kOutput, calls=%fused_computation.76 | convolution fusion | flops 402653184 | bytes 4390912 | tf_op jit(solution)/shard_map/dot_general | solution.py:507
  145.6 5.7 %add_convert_fusion = bf16[384,2048]{1,0:T(8,128)(2,1)} fusion(f32[384,2048]{1,0:T(8,128)} %fusion.43, bf16[128,2048]{1,0:T(8,128)(2,1)} %param.30, bf16[2048,128]{1,0:T(8,128)(2,1)} %param.18, bf16[384,2048]{1,0:T(8,128)(2,1)} %gather_tp.1, f32[2048]{0:T(1024)S(1)} %copy-done.7, bf16[384,128]{1,0:T(8,128)(2,1)S(1)} %copy-done.6, ...), kind=kOutput, calls=%fused_computation.5 | convolution fusion | flops 407519232 | bytes 7450112 | tf_op jit(solution)/shard_map/dot_general | solution.py:510
  151.3 1.5 copy.31
  152.8 25.2 %all_to_all.11 = bf16[8,384,256]{2,1,0:T(8,128)(2,1)S(1)} all-to-all(bf16[8,384,256]{2,1,0:T(8,128)(2,1)S(1)} %bitcast.39), channel_id=1, replica_groups=mesh['sp'=32,'tp'=8] {'tp'}, dimensions={0} | all-to-all | bytes 3145728 | tf_op jit(solution)/shard_map/all_to_all | solution.py:407
  179.0 3.3 %all-to-all-start.1 = ((f32[8,1,384]{2,1,0:T(1,128)}), f32[8,1,384]{2,1,0:T(1,128)S(1)}, u32[]{:S(2)}, u32[]{:S(2)}) async-start(f32[8,1,384]{2,1,0:T(1,128)} %broadcast_in_dim.5), calls=%async_computation.1 | async-start | bytes 24576 | tf_op jit(solution)/shard_map/all_to_all | solution.py:388
  183.7 3.9 %all-to-all-done.1 = f32[8,1,384]{2,1,0:T(1,128)S(1)} async-done(((f32[8,1,384]{2,1,0:T(1,128)}), f32[8,1,384]{2,1,0:T(1,128)S(1)}, u32[]{:S(2)}, u32[]{:S(2)}) %all-to-all-start.1) | async-done | bytes 12320 | tf_op jit(solution)/shard_map/all_to_all | solution.py:388
  187.6 1.5 multiply_convert_fusion.4
  (46 shorter events, 6.4 us)
Async XLA Ops:
  0.6 25.6 %copy-start = (bf16[2048,768]{1,0:T(8,128)(2,1)S(1)}, bf16[2048,768]{1,0:T(8,128)(2,1)}, u32[]{:S(2)}) copy-start(bf16[2048,768]{1,0:T(8,128)(2,1)} %param.22) | copy-start | bytes 9437188
  0.6 17.8 %copy-start.7 = (f32[2048]{0:T(1024)S(1)}, f32[2048]{0:T(1024)}, u32[]{:S(2)}) copy-start(f32[2048]{0:T(1024)} %param.17) | copy-start | bytes 24580
  16.5 2.0 %copy-start.1 = (bf16[384,2048]{1,0:T(8,128)(2,1)S(1)}, bf16[384,2048]{1,0:T(8,128)(2,1)}, u32[]{:S(2)}) copy-start(bf16[384,2048]{1,0:T(8,128)(2,1)} %gather_tp.1) | copy-start | bytes 4718596
  18.4 1.7 copy-start.11
  20.8 0.7 copy-start.5
  21.9 123.6 %collective-permute-start = (bf16[2,128]{1,0:T(2,128)(2,1)}, bf16[2,128]{1,0:T(2,128)(2,1)}, u32[]{:S(2)}, u32[]{:S(2)}) collective-permute-start(bf16[2,128]{1,0:T(2,128)(2,1)} %slice.67), channel_id=1, source_target_pairs={{0,8},{8,16},{16,24},{24,32},{32,40},{40,48},{48,56},{56,64},{64,7... | collective-permute-start | bytes 1544 | tf_op jit(solution)/shard_map/ppermute | solution.py:396
  26.2 2.4 %copy-start.12 = (bf16[2048,32]{0,1:T(8,128)(2,1)S(1)}, bf16[2048,32]{0,1:T(8,128)(2,1)}, u32[]{:S(2)}) copy-start(bf16[2048,32]{0,1:T(8,128)(2,1)} %param.26) | copy-start | bytes 393220
  28.6 1.2 copy-start.8
  29.8 3.7 %copy-start.2 = (bf16[384,2048]{1,0:T(8,128)(2,1)S(1)}, bf16[384,2048]{1,0:T(8,128)(2,1)}, u32[]{:S(2)}) copy-start(bf16[384,2048]{1,0:T(8,128)(2,1)} %gather_tp.1) | copy-start | bytes 4718596
  32.0 0.8 copy-start.3
  33.5 2.7 %copy-start.4 = (bf16[512,512]{1,0:T(8,128)(2,1)S(1)}, bf16[512,512]{1,0:T(8,128)(2,1)}, u32[]{:S(2)}) copy-start(bf16[512,512]{1,0:T(8,128)(2,1)} %param.28) | copy-start | bytes 1572868
  33.5 2.7 %copy-start.10 = (f32[512]{0:T(512)S(1)}, f32[512]{0:T(512)}, u32[]{:S(2)}) copy-start(f32[512]{0:T(512)} %param.27) | copy-start | bytes 6148
  141.9 3.6 %copy-start.9 = (bf16[3,128]{1,0:T(4,128)(2,1)S(1)}, bf16[3,128]{1,0:T(4,128)(2,1)}, u32[]{:S(2)}) copy-start(bf16[3,128]{1,0:T(4,128)(2,1)} %param.21) | copy-start | bytes 2308
  141.9 3.6 %copy-start.6 = (bf16[384,128]{1,0:T(8,128)(2,1)S(1)}, bf16[384,128]{1,0:T(8,128)(2,1)}, u32[]{:S(2)}) copy-start(bf16[384,128]{1,0:T(8,128)(2,1)} %copy-done.5) | copy-start | bytes 294916
  179.0 8.6 %all-to-all-start.1 = ((f32[8,1,384]{2,1,0:T(1,128)}), f32[8,1,384]{2,1,0:T(1,128)S(1)}, u32[]{:S(2)}, u32[]{:S(2)}) async-start(f32[8,1,384]{2,1,0:T(1,128)} %broadcast_in_dim.5), calls=%async_computation.1 | async-start | bytes 24576 | tf_op jit(solution)/shard_map/all_to_all | solution.py:388
